TPU v7x, 32 devices: a whole 2x2x4 slice. The times are simulated.
32 devices in a mesh: ep: 8 (over z, x), tp: 4 (over y, core).
Axes of the slice: x: 2, y: 2, z: 4, core: 2. Of those that a mesh axis runs over, the one named last changes fastest.
Arguments:
- query_logits: bfloat16 [2048, 2048], P('ep', 'tp'), may hold values from -6 to 6
- forget_gate_logits: bfloat16 [2048, 2048], P('ep', 'tp'), may hold values from -3.75 to 3.75
- written_values: bfloat16 [2048, 2048], P('ep', 'tp'), may hold values from -6 to 6
- output_gate_logits: bfloat16 [2048, 2048], P('ep', 'tp'), may hold values from -6 to 6
- gap: float32 [2048], P('tp'), may hold values from 4.8828125e-05 to 0.06
- extra_log_forget: float32 [2048, 2048], P('ep', 'tp'), may hold values from -0.7 to 0
- head_norm_scale: float32 [2048], P('tp'), may hold values from 0.1 to 1.9
- mixer_output_matrix: bfloat16 [2048, 2048], P('tp'), may hold values from -0.125 to 0.125
- expert_input_tokens: bfloat16 [2048, 2048], P('ep'), may hold values from -12 to 12
- expert_norm_scale: float32 [2048], replicated, may hold values from 0.1 to 1.9
- routes: int32 [2048, 2], P('ep'), may hold values from 0 to 7, all different within a row; in each aligned block of 256 rows (0 to 255, 256 to 511, ...) at most 96 rows name the same one
- router_scores_chosen: float32 [2048, 2], P('ep'), may hold values from -6 to 6
- expert_gate_matrix: bfloat16 [8, 2048, 4096], P('ep', None, 'tp'), may hold values from -0.125 to 0.125
- expert_up_matrix: bfloat16 [8, 2048, 4096], P('ep', None, 'tp'), may hold values from -0.125 to 0.125
- expert_down_matrix: bfloat16 [8, 2048, 4096], P('ep', None, 'tp'), may hold values from -0.09375 to 0.09375
Outputs:
- mixer_output_rows: bfloat16 [2048, 2048], P(('ep', 'tp'))
- expert_out: bfloat16 [2048, 2048], P('ep', 'tp')
Inputs may be any that keep to these rules, and one draw needn't show every extreme that they name: `routes`: each row names two different experts. Among the rows of one device no expert is named more than 96 times, and 96 is reached in some blocks.
All inputs are finite; a program needn't handle non-finite values.
Results may differ from a plain program's by a relative error of at most 0.019.
Values may be sent and summed in bfloat16 or wider, within the bound.
A program may use at most 64 MiB of HBM per device.

v0:
```python
import jax
import jax.numpy as jnp
from jax import lax
from jax.sharding import PartitionSpec as P

HEAD_DIM = 128


exact_precision = lax.Precision.HIGHEST


def entering(x, axis, join, neutral):
    place = lax.axis_index(axis)
    gathered = jax.tree.map(
        lambda a, kind: lax.all_gather(a.astype(kind), axis), x, (jnp.bfloat16, jnp.bfloat16)
    )
    state = jax.tree.map(lambda a, e: jnp.zeros_like(a) + jnp.asarray(e, a.dtype), x, neutral)

    def one(hop, state):
        return join(
            state,
            jax.tree.map(
                lambda a, own: lax.dynamic_index_in_dim(a, hop, 0, False).astype(own.dtype),
                gathered,
                x,
            ),
        )

    return lax.fori_loop(0, place, one, state)


def join_states(earlier, later):
    decay_early, state_early = earlier
    decay_late, state_late = later
    return (decay_early * decay_late, decay_late[..., None] * state_early + state_late)


def mixer_half(
    query_logits,
    forget_gate_logits,
    written_values,
    output_gate_logits,
    gap,
    extra_log_forget,
    head_norm_scale,
    mixer_output_matrix,
):
    tokens, channels = query_logits.shape
    local_heads = channels // HEAD_DIM
    final_result = gap * jax.nn.sigmoid(-forget_gate_logits.astype(jnp.float32))
    decay_logarithm = jnp.log1p(-final_result) + extra_log_forget
    queries = jax.nn.silu(query_logits.astype(jnp.float32))
    values = written_values.astype(jnp.float32)

    def by_head(array):
        return array.reshape(tokens, local_heads, HEAD_DIM).transpose(1, 0, 2)

    final_result, decay_logarithm, queries, values = (
        by_head(final_result),
        by_head(decay_logarithm),
        by_head(queries),
        by_head(values),
    )
    running = jnp.cumsum(decay_logarithm, axis=1)
    query_decayed = queries * jnp.exp(running)
    key_decayed = final_result * jnp.exp(-running)
    scores = jnp.einsum("htd,hsd->hts", query_decayed, key_decayed, precision=exact_precision)
    causal = jnp.arange(tokens)[:, None] >= jnp.arange(tokens)[None, :]
    scores = jnp.where(causal[None], scores, 0.0)
    within = jnp.einsum("hts,hsv->htv", scores, values, precision=exact_precision)
    ending = running[:, -1:, :]
    key_state = final_result * jnp.exp(ending - running)
    end_state = jnp.einsum("htd,htv->hdv", key_state, values, precision=exact_precision)
    span_decay = jnp.exp(ending[:, 0, :])
    identity = (jnp.ones_like(span_decay), jnp.zeros_like(end_state))
    _, incoming = entering((span_decay, end_state), "ep", join_states, identity)
    carried = jnp.einsum("htd,hdv->htv", query_decayed, incoming, precision=exact_precision)
    recurrent = within + carried
    scaled = recurrent * lax.rsqrt(jnp.mean(recurrent * recurrent, axis=-1, keepdims=True) + 1e-06)
    scaled = scaled.transpose(1, 0, 2).reshape(tokens, channels)
    hidden = (
        scaled * head_norm_scale * jax.nn.silu(output_gate_logits.astype(jnp.float32))
    ).astype(jnp.bfloat16)
    return lax.psum_scatter(
        jnp.dot(hidden, mixer_output_matrix, preferred_element_type=jnp.float32).astype(
            jnp.bfloat16
        ),
        "tp",
        scatter_dimension=0,
        tiled=True,
    )


def expert_half(
    expert_input_tokens,
    expert_norm_scale,
    routes,
    router_scores_chosen,
    expert_gate_matrix,
    expert_up_matrix,
    expert_down_matrix,
):
    tokens, channels = expert_input_tokens.shape
    experts = lax.axis_size("ep")
    capacity = 3 * tokens // experts
    inputs32 = expert_input_tokens.astype(jnp.float32)
    centred = inputs32 - jnp.mean(inputs32, axis=-1, keepdims=True)
    variance = jnp.mean(centred * centred, axis=-1, keepdims=True)
    normed = (centred * lax.rsqrt(variance + 1e-05) * expert_norm_scale).astype(jnp.bfloat16)
    first_weight = jax.nn.sigmoid(router_scores_chosen[:, 0] - router_scores_chosen[:, 1])
    route_weight = jnp.stack([first_weight, 1.0 - first_weight], axis=1)
    flat_routes = routes.reshape(-1)
    onehot = (flat_routes[:, None] == jnp.arange(experts, dtype=jnp.int32)[None, :]).astype(
        jnp.int32
    )
    earlier = jnp.cumsum(onehot, axis=0) - onehot
    position = jnp.sum(earlier * onehot, axis=1)
    target = flat_routes * capacity + position
    token_ids = jnp.arange(2 * tokens, dtype=jnp.int32) // 2
    owner = jnp.zeros((experts * capacity,), jnp.int32).at[target].set(token_ids)
    filled = jnp.zeros((experts * capacity,), jnp.bool_).at[target].set(True)
    local_gate = expert_gate_matrix[0]
    local_up = expert_up_matrix[0]
    local_down = expert_down_matrix[0]
    slice_width = channels // lax.axis_size("tp")
    own_columns = lax.dynamic_slice_in_dim(
        normed, lax.axis_index("tp") * slice_width, slice_width, 1
    )
    outgoing = jnp.where(filled[:, None], own_columns[owner], jnp.zeros((), jnp.bfloat16))
    arrived = lax.all_to_all(outgoing, "ep", split_axis=0, concat_axis=0, tiled=True)
    features = lax.all_gather(arrived, "tp", axis=1, tiled=True)
    gate_act = jnp.dot(features, local_gate, preferred_element_type=jnp.float32)
    up_act = jnp.dot(features, local_up, preferred_element_type=jnp.float32)
    hidden = (jax.nn.silu(gate_act) * up_act).astype(jnp.bfloat16)
    summed = lax.psum_scatter(
        lax.dot_general(
            local_down, hidden, (((1,), (1,)), ((), ())), preferred_element_type=jnp.float32
        ).astype(jnp.bfloat16),
        "tp",
        scatter_dimension=0,
        tiled=True,
    )
    returned = lax.all_to_all(summed, "ep", split_axis=1, concat_axis=1, tiled=True)
    chosen = returned.T[target].astype(jnp.float32).reshape(tokens, 2, -1)
    return jnp.sum(chosen * route_weight[:, :, None], axis=1).astype(jnp.bfloat16)


def body(
    query_logits,
    forget_gate_logits,
    written_values,
    output_gate_logits,
    gap,
    extra_log_forget,
    head_norm_scale,
    mixer_output_matrix,
    expert_input_tokens,
    expert_norm_scale,
    routes,
    router_scores_chosen,
    expert_gate_matrix,
    expert_up_matrix,
    expert_down_matrix,
):
    mixer_output_rows = mixer_half(
        query_logits,
        forget_gate_logits,
        written_values,
        output_gate_logits,
        gap,
        extra_log_forget,
        head_norm_scale,
        mixer_output_matrix,
    )
    expert_out = expert_half(
        expert_input_tokens,
        expert_norm_scale,
        routes,
        router_scores_chosen,
        expert_gate_matrix,
        expert_up_matrix,
        expert_down_matrix,
    )
    return (mixer_output_rows, expert_out)


def solution(mesh):
    return jax.shard_map(
        body,
        mesh=mesh,
        in_specs=(
            P("ep", "tp"),
            P("ep", "tp"),
            P("ep", "tp"),
            P("ep", "tp"),
            P("tp"),
            P("ep", "tp"),
            P("tp"),
            P("tp", None),
            P("ep", None),
            P(),
            P("ep", None),
            P("ep", None),
            P("ep", None, "tp"),
            P("ep", None, "tp"),
            P("ep", None, "tp"),
        ),
        out_specs=(P(("ep", "tp"), None), P("ep", "tp")),
        check_vma=False,
    )
```

profile of v0, /device:TPU:0, one launch (start us, length us, event | category | flops | bytes accessed | tf_op | source)
XLA Modules:
  0.0 200.6 jit_solution(9134592011714128732)
XLA Ops:
  9.2 1.4 convert_reduce_fusion
  10.6 2.9 %multiply_reduce_fusion = (f32[256]{0:T(256)S(1)}, f32[256,2048]{1,0:T(8,128)}) fusion(f32[256]{0:T(256)S(1)} %broadcast_multiply_fusion.1, bf16[256,2048]{1,0:T(8,128)(2,1)} %param.25), kind=kLoop, calls=%fused_computation.18 | loop fusion | flops 2096896 | bytes 3147776 | tf_op jit(solution)/shard_map/reduce_sum | solution.py:108
  15.3 2.4 %scatter_custom_fusion.1 = s32[768]{0:T(1024)S(1)} fusion(s32[512]{0:T(512)S(1)} %bitcast.121, s32[512]{0:T(512)S(1)} %add_select_fusion, s32[]{:T(128)} %constant.71.clone.1), kind=kCustom, calls=%fused_computation.80 | custom fusion | bytes 3076 | tf_op jit(solution)/shard_map/scatter | solution.py:120
  17.8 2.4 %scatter_custom_fusion = pred[768]{0:T(1024)(128)(4,1)S(1)} fusion(s32[512]{0:T(512)S(1)} %bitcast.122, pred[512]{0:T(512)(128)(4,1)S(1)} %broadcast.132, pred[]{:T(512)} %constant.76.clone.1), kind=kCustom, calls=%fused_computation.84 | custom fusion | bytes 769 | tf_op jit(solution)/shard_map/scatter | solution.py:121
  22.3 2.7 %gather_fusion = bf16[768,512]{1,0:T(8,128)(2,1)S(1)} fusion(bf16[256,512]{1,0:T(8,128)(2,1)S(1)} %fusion.22, s32[1024]{0:T(1024)S(1)} %pad_clamp_fusion.1), kind=kCustom, calls=%fused_computation | custom fusion | bytes 1575936 | tf_op jit(solution)/shard_map/gather | solution.py:129
  25.2 27.3 %all_to_all.21 = bf16[8,96,512]{2,1,0:T(8,128)(2,1)} all-to-all(bf16[8,96,512]{2,1,0:T(8,128)(2,1)S(1)} %broadcast_select_fusion), channel_id=1, replica_groups=mesh['ep'=8,'tp'=4] {'ep'}, dimensions={0} | all-to-all | bytes 1572864 | tf_op jit(solution)/shard_map/all_to_all | solution.py:130
  58.1 2.1 %copy.99 = f32[256,4,128]{2,1,0:T(4,128)} copy(f32[256,4,128]{0,2,1:T(8,128)} %bitcast.115) | data formatting | bytes 1048576 | tf_op jit(solution)/shard_map/reshape | solution.py:56
  60.3 1.8 copy.91
  64.9 2.7 %bitcast_multiply_fusion.3 = (f32[4,256,128]{2,0,1:T(4,128)}, f32[4,256,128]{2,0,1:T(4,128)S(1)}, f32[4,256,128]{2,0,1:T(4,128)S(1)}) fusion(f32[256,4,128]{2,1,0:T(4,128)} %copy.99, f32[4,128,256]{1,2,0:T(8,128)S(1)} %bitcast.110, f32[4,128]{1,0:T(4,128)S(1)} %get-tuple-element.64, f32[256,4,128]{2,1,0:T(4,128)} %copy.92), kind=kLoop, calls=%fused_computation.41 | loop fusion | flops 655360 | bytes 3147776 | tf_op jit(solution)/shard_map/mul | solution.py:66
  69.1 11.1 %all-gather.5.cloned.1.call-done = bf16[768,2048]{1,0:T(8,128)(2,1)} async-done(((bf16[768,512]{1,0:T(8,128)(2,1)}), bf16[768,2048]{1,0:T(8,128)(2,1)}) %all-gather.5.cloned.1.call-update) | async-done | bytes 3145744 | tf_op jit(solution)/shard_map/all_gather | solution.py:131
  80.2 6.3 %fusion.2 = f32[768,1024]{1,0:T(8,128)S(1)} fusion(bf16[768,2048]{1,0:T(8,128)(2,1)} %all-gather.5.cloned.1.call-done, bf16[1,2048,1024]{2,1,0:T(8,128)(2,1)} %param.30), kind=kOutput, calls=%fused_computation.8 | convolution fusion | flops 3221225472 | bytes 10485760 | tf_op jit(solution)/shard_map/dot_general | solution.py:133
  86.6 3.8 %multiply_convert_fusion = bf16[768,1024]{1,0:T(8,128)(2,1)S(1)} fusion(f32[768,1024]{1,0:T(8,128)S(1)} %fusion.2, bf16[768,2048]{1,0:T(8,128)(2,1)S(1)} %copy-done.9, bf16[1,2048,1024]{2,1,0:T(8,128)(2,1)S(1)} %copy-done.7), kind=kOutput, calls=%fused_computation.13 | convolution fusion | flops 3225944064 | bytes 12058624 | tf_op jit(solution)/shard_map/dot_general | solution.py:132
  90.4 4.9 %fusion.9 = bf16[2048,768]{0,1:T(8,128)(2,1)} fusion(bf16[768,1024]{1,0:T(8,128)(2,1)S(1)} %multiply_convert_fusion, bf16[1,2048,1024]{2,1,0:T(8,128)(2,1)S(1)} %copy-done.8), kind=kOutput, calls=%fused_computation.14 | convolution fusion | flops 3222798336 | bytes 8912896 | tf_op jit(solution)/shard_map/dot_general | solution.py:136
  95.4 26.8 %all-gather = bf16[32,1,128]{2,1,0:T(2,128)(2,1)S(1)} all-gather(bf16[4,1,128]{2,1,0:T(2,128)(2,1)S(1)} %copy.104), channel_id=2, replica_groups=mesh['ep'=8,'tp'=4] {'ep'}, dimensions={0}, use_global_device_ids=true | all-gather | bytes 9216 | tf_op jit(solution)/shard_map/all_gather | solution.py:15
  122.2 1.8 copy.108
  124.0 2.0 convolution_select_fusion
  126.7 2.0 multiply_reduce_fusion.2
  129.0 1.7 convolution_convert_fusion
  130.7 31.4 %reduce-scatter.5.cloned.1.call-done = bf16[512,768]{0,1:T(8,128)(2,1)} async-done(((bf16[2048,768]{0,1:T(8,128)(2,1)}), bf16[512,768]{0,1:T(8,128)(2,1)}) %reduce-scatter.5.cloned.1.call-update) | async-done | bytes 786448 | tf_op jit(solution)/shard_map/reduce_scatter | solution.py:135
  162.1 5.5 %all-to-all-start.1 = ((bf16[512,8,96]{0,2,1:T(8,128)(2,1)}), bf16[512,8,96]{0,2,1:T(8,128)(2,1)S(1)}, u32[]{:S(2)}, u32[]{:S(2)}) async-start(bf16[512,8,96]{0,2,1:T(8,128)(2,1)} %bitcast.117), calls=%async_computation.3 | async-start | bytes 1572864 | tf_op jit(solution)/shard_map/all_to_all | solution.py:143
  167.8 19.9 %all-to-all-done.1 = bf16[512,8,96]{0,2,1:T(8,128)(2,1)S(1)} async-done(((bf16[512,8,96]{0,2,1:T(8,128)(2,1)}), bf16[512,8,96]{0,2,1:T(8,128)(2,1)S(1)}, u32[]{:S(2)}, u32[]{:S(2)}) %all-to-all-start.1) | async-done | bytes 786464 | tf_op jit(solution)/shard_map/all_to_all | solution.py:143
  187.7 2.6 %gather_fusion.1 = bf16[512,512]{1,0:T(8,128)(2,1)} fusion(bf16[768,512]{1,0:T(8,128)(2,1)S(1)} %bitcast.108, s32[1024]{0:T(1024)S(1)} %pad_clamp_fusion), kind=kCustom, calls=%fused_computation.1 | custom fusion | bytes 1050624 | tf_op jit(solution)/shard_map/gather | solution.py:144
  190.3 1.7 reshape.160
  192.0 2.1 %multiply_reduce_fusion.1 = bf16[256,512]{1,0:T(8,128)(2,1)} fusion(f32[256,2,512]{2,1,0:T(2,128)S(1)} %reshape.160, f32[256,2]{1,0:T(8,128)S(1)} %copy.112), kind=kLoop, calls=%fused_computation.22 | loop fusion | flops 393216 | bytes 1312768 | tf_op jit(solution)/shard_map/reduce_sum | solution.py:145
  (81 shorter events, 17.1 us)
Async XLA Ops:
  7.2 121.8 %copy-start = (bf16[512,2048]{1,0:T(8,128)(2,1)S(1)}, bf16[512,2048]{1,0:T(8,128)(2,1)}, u32[]{:S(2)}) copy-start(bf16[512,2048]{1,0:T(8,128)(2,1)} %param.24) | copy-start | bytes 6291460
  7.2 73.0 %all-gather.5.cloned.1.call-start = ((), (), s32[]{:S(2)}) async-start(), calls=%async_computation.5 | async-start | bytes 3932160 | tf_op jit(solution)/shard_map/all_gather | solution.py:131
  25.0 29.9 %copy-start.6 = (f32[512]{0:T(512)S(1)}, f32[512]{0:T(512)}, u32[]{:S(2)}) copy-start(f32[512]{0:T(512)} %param.21) | copy-start | bytes 6148
  52.5 73.5 %all-gather.7.cloned.1.call-start = ((), (), s32[]{:S(2)}) async-start(), calls=%async_computation.7 | async-start | bytes 1179648 | tf_op jit(solution)/shard_map/all_gather | solution.py:15
  58.1 9.5 %copy-start.2 = (bf16[256,512]{1,0:T(8,128)(2,1)S(1)}, bf16[256,512]{1,0:T(8,128)(2,1)}, u32[]{:S(2)}) copy-start(bf16[256,512]{1,0:T(8,128)(2,1)} %param.19) | copy-start | bytes 786436
  68.9 93.2 %reduce-scatter.5.cloned.1.call-start = ((), (), s32[]{:S(2)}) async-start(), calls=%async_computation.6 | async-start | bytes 3932160 | tf_op jit(solution)/shard_map/reduce_scatter | solution.py:135
  80.2 6.3 %copy-start.7 = (bf16[1,2048,1024]{2,1,0:T(8,128)(2,1)S(1)}, bf16[1,2048,1024]{2,1,0:T(8,128)(2,1)}, u32[]{:S(2)}) copy-start(bf16[1,2048,1024]{2,1,0:T(8,128)(2,1)} %param.29) | copy-start | bytes 12582916
  80.2 6.3 %copy-start.9 = (bf16[768,2048]{1,0:T(8,128)(2,1)S(1)}, bf16[768,2048]{1,0:T(8,128)(2,1)}, u32[]{:S(2)}) copy-start(bf16[768,2048]{1,0:T(8,128)(2,1)} %all-gather.5.cloned.1.call-done) | copy-start | bytes 9437188
  86.5 3.8 %copy-start.8 = (bf16[1,2048,1024]{2,1,0:T(8,128)(2,1)S(1)}, bf16[1,2048,1024]{2,1,0:T(8,128)(2,1)}, u32[]{:S(2)}) copy-start(bf16[1,2048,1024]{2,1,0:T(8,128)(2,1)} %param.31) | copy-start | bytes 12582916
  95.3 28.7 %copy-start.1 = (f32[4,256,128]{2,0,1:T(4,128)S(1)}, f32[4,256,128]{2,0,1:T(4,128)}, u32[]{:S(2)}) copy-start(f32[4,256,128]{2,0,1:T(4,128)} %get-tuple-element.61) | copy-start | bytes 1572868
  95.3 98.8 %reduce-scatter.3.cloned.1.call-start = ((), (), s32[]{:S(2)}) async-start(), calls=%async_computation.4 | async-start | bytes 1310720 | tf_op jit(solution)/shard_map/reduce_scatter | solution.py:84
  126.1 2.7 %copy-start.3 = (bf16[256,512]{0,1:T(8,128)(2,1)S(1)}, bf16[256,512]{0,1:T(8,128)(2,1)}, u32[]{:S(2)}) copy-start(bf16[256,512]{0,1:T(8,128)(2,1)} %copy.108) | copy-start | bytes 786436
  126.1 2.7 %copy-start.4 = (f32[512]{0:T(512)S(1)}, f32[512]{0:T(512)}, u32[]{:S(2)}) copy-start(f32[512]{0:T(512)} %param.23) | copy-start | bytes 6148
  129.0 38.7 %copy-start.5 = (f32[256,2]{0,1:T(2,128)S(1)}, f32[256,2]{0,1:T(2,128)}, u32[]{:S(2)}) copy-start(f32[256,2]{0,1:T(2,128)} %param.28) | copy-start | bytes 6148
  162.1 25.6 %all-to-all-start.1 = ((bf16[512,8,96]{0,2,1:T(8,128)(2,1)}), bf16[512,8,96]{0,2,1:T(8,128)(2,1)S(1)}, u32[]{:S(2)}, u32[]{:S(2)}) async-start(bf16[512,8,96]{0,2,1:T(8,128)(2,1)} %bitcast.117), calls=%async_computation.3 | async-start | bytes 1572864 | tf_op jit(solution)/shard_map/all_to_all | solution.py:143
Sparse Core Ops, SparseCore 0:
  52.6 27.5 all-gather.4
  82.9 40.3 all-gather.6
  125.8 36.2 reduce-scatter.4
  165.1 24.7 reduce-scatter.2
where the time goes:
time: 201 us
  waiting for transfers between devices  62.5 us (31%)
  blocking collectives  54.2 us (27%)
  local copies, waits for them, and re-layouts  25.1 us (12%)
  matrix products  22.6 us (11%)
  other arithmetic  16.3 us (8%)
  between operations  14.1 us (7%)
  starting transfers between devices  5.85 us (3%)
    reduce_scatter x1, waiting for transfers between devices, expert_half(): lax.psum_scatter(lax.dot_general(local_down, hidden, (((1,), (1,)), ((),...  31.4 us
    all_to_all x1, blocking collectives, expert_half(): lax.all_to_all(outgoing, 'ep', split_axis=0, concat_axis=0, tiled=True)  27.3 us
    all_gather x1, blocking collectives, entering(): lax.all_gather(a.astype(kind), axis)  26.8 us
    all_to_all x1, waiting for transfers between devices, expert_half(): lax.all_to_all(summed, 'ep', split_axis=1, concat_axis=1, tiled=True)  19.9 us
    all_gather x1, waiting for transfers between devices, expert_half(): features = lax.all_gather(arrived, 'tp', axis=1, tiled=True)  11.1 us
    unnamed x26, local copies, waits for them, and re-layouts  6.94 us
    dot_general x1, matrix products, expert_half(): up_act = jnp.dot(features, local_up, preferred_element_type=jnp.float32)  6.28 us
    all_to_all x1, starting transfers between devices, expert_half(): lax.all_to_all(summed, 'ep', split_axis=1, concat_axis=1, tiled=True)  5.51 us
  transfers between devices with their start and end apart: 5, of which 3 were waited for; matrix products, arithmetic and copies ran while one was open for 23% of the time, Pallas kernels for 0%

commit v1 on v0

v1 whole, which is shorter than its diff:
```python
import functools

import jax
import jax.numpy as jnp
from jax import lax
from jax.experimental import pallas as pl
from jax.experimental.pallas import tpu as pltpu
from jax.sharding import PartitionSpec as P

HEAD_DIM = 128
CHUNK = 64
MESH = pl.DeviceIdType.MESH
F32 = jnp.float32
BF16 = jnp.bfloat16


def flip(i, k):
    b = 1
    while b <= k:
        if k & b:
            i = i + b - 2 * b * lax.rem(lax.div(i, b), 2)
        b *= 2
    return i


def kernel(
    E, T, cap, pieces,
    q_ref, f_ref, v_ref, o_ref, gap_ref, extra_ref, hscale_ref,
    mixw_hbm, tok_ref, escale_ref, routes_ref, scores_ref,
    gate_hbm, up_hbm, down_hbm,
    mix_out, exp_out,
    gate, up, down, mixw,
    ncols, dmat, wmat, outgoing, feats, hidden, part, precv, xsend, xrecv, fin, ret,
    qs, ks, run, qg, rec, ist, idec, est, edec, ksend, krecv,
    mhid, mpart, mprecv, mxsend, mxrecv,
    wsem, send_sem, recv_sem,
):
    me = lax.axis_index("ep")
    t = lax.axis_index("tp")
    G = T // 2
    g, c = lax.div(t, 2), lax.rem(t, 2)
    oc = 1 - c
    tokens, width = q_ref.shape
    heads = width // HEAD_DIM
    S = E * cap
    Dl = ncols.shape[1]
    FFl = hidden.shape[1]

    loads = [
        pltpu.make_async_copy(src, dst, wsem.at[i])
        for i, (src, dst) in enumerate(
            ((gate_hbm, gate), (up_hbm, up), (down_hbm, down), (mixw_hbm, mixw))
        )
    ]
    for load in loads:
        load.start()

    barrier = pltpu.get_barrier_semaphore()
    for k in range(1, E):
        pl.semaphore_signal(barrier, inc=1, device_id=(flip(me, k), t), device_id_type=MESH)
    pl.semaphore_signal(barrier, inc=1, device_id=(me, 2 * g + oc), device_id_type=MESH)
    for j in range(1, G):
        pl.semaphore_signal(
            barrier, inc=1, device_id=(me, 2 * flip(g, j) + c), device_id_type=MESH
        )

    used = [0]

    def remote(src, dst, device):
        slot = used[0]
        used[0] += 1
        return pltpu.make_async_remote_copy(
            src_ref=src, dst_ref=dst, send_sem=send_sem.at[slot], recv_sem=recv_sem.at[slot],
            device_id=device, device_id_type=MESH,
        )

    def arrival(src, dst, copy_slot):
        return pltpu.make_async_remote_copy(
            src_ref=src, dst_ref=dst, send_sem=send_sem.at[copy_slot],
            recv_sem=recv_sem.at[copy_slot], device_id=(me, t), device_id_type=MESH,
        )

    sent = []

    x = tok_ref[...].astype(F32)
    mean = jnp.mean(x, axis=-1, keepdims=True)
    centred = x - mean
    inv = lax.rsqrt(jnp.mean(centred * centred, axis=-1, keepdims=True) + 1e-05)
    cols = pl.ds(pl.multiple_of(t * Dl, 128), Dl)
    ncols[...] = ((tok_ref[:, cols].astype(F32) - mean) * inv * escale_ref[:, cols]).astype(BF16)

    ntok = tok_ref.shape[0]
    ek = lax.broadcasted_iota(jnp.int32, (E, ntok), 0) ^ me
    first, second = routes_ref[0:1, :] == ek, routes_ref[1:2, :] == ek
    named = jnp.where(first | second, 1.0, 0.0)
    earlier = jnp.where(
        lax.broadcasted_iota(jnp.int32, (ntok, ntok), 0)
        < lax.broadcasted_iota(jnp.int32, (ntok, ntok), 1), 1.0, 0.0
    ).astype(BF16)
    position = jnp.dot(named.astype(BF16), earlier, preferred_element_type=F32)
    place = jnp.where(first | second, position, -1.0).astype(jnp.int32)
    w0 = jax.nn.sigmoid(scores_ref[0:1, :] - scores_ref[1:2, :])
    weight = jnp.where(first, w0, jnp.where(second, 1.0 - w0, 0.0))
    rows = lax.broadcasted_iota(jnp.int32, (cap, ntok), 0)
    for k in range(E):
        hit = rows == place[k:k + 1, :]
        dmat[k * cap:(k + 1) * cap, :] = jnp.where(hit, 1.0, 0.0).astype(BF16)
        wmat[k * cap:(k + 1) * cap, :] = jnp.where(hit, weight[k:k + 1, :], 0.0).astype(BF16)
    outgoing[...] = jnp.dot(dmat[...], ncols[...], preferred_element_type=F32).astype(BF16)
    feats[t, 0:cap, :] = outgoing[0:cap, :]

    pl.semaphore_wait(barrier, E - 1 + 1 + G - 1)

    dispatch = {}
    for k in range(1, E):
        block = pl.ds(k * cap, cap)
        dispatch[k] = remote(outgoing.at[block], feats.at[t, block], (flip(me, k), t))
        dispatch[k].start()
        sent.append(dispatch[k])

    closing = gap_ref[...] * jax.nn.sigmoid(-f_ref[...].astype(F32))
    ks[...] = closing
    logd = jnp.log1p(-closing) + extra_ref[...]
    qs[...] = jax.nn.silu(q_ref[...].astype(F32))
    r_i = lax.broadcasted_iota(jnp.int32, (CHUNK, CHUNK), 0)
    c_i = lax.broadcasted_iota(jnp.int32, (CHUNK, CHUNK), 1)
    causal = r_i >= c_i
    tri = jnp.where(causal, 1.0, 0.0).astype(F32)
    nchunks = tokens // CHUNK
    for n in range(nchunks):
        run[n * CHUNK:(n + 1) * CHUNK, :] = jnp.dot(
            tri, logd[n * CHUNK:(n + 1) * CHUNK, :], precision=lax.Precision.HIGHEST,
            preferred_element_type=F32,
        )

    def head_local(h, _):
        lanes = pl.ds(pl.multiple_of(h * HEAD_DIM, HEAD_DIM), HEAD_DIM)
        state = jnp.zeros((HEAD_DIM, HEAD_DIM), F32)
        before = jnp.zeros((1, HEAD_DIM), F32)
        for n in range(nchunks):
            rs = slice(n * CHUNK, (n + 1) * CHUNK)
            r = run[rs, lanes]
            total = r[CHUNK - 1:CHUNK, :]
            qd = qs[rs, lanes] * jnp.exp(r)
            key = ks[rs, lanes]
            kd = (key * jnp.exp(-r)).astype(BF16)
            kst = (key * jnp.exp(total - r)).astype(BF16)
            val = v_ref[rs, lanes]
            qd_b = qd.astype(BF16)
            scores = lax.dot_general(
                qd_b, kd, (((1,), (1,)), ((), ())), preferred_element_type=F32
            )
            scores = jnp.where(causal, scores, 0.0).astype(BF16)
            out = jnp.dot(scores, val, preferred_element_type=F32)
            if n:
                out += lax.dot_general(
                    qd_b, state.astype(BF16), (((1,), (1,)), ((), ())),
                    preferred_element_type=F32,
                )
            rec[rs, lanes] = out
            qg[rs, lanes] = (qd * jnp.exp(before)).astype(BF16)
            state = state * jnp.exp(total) + lax.dot_general(
                val, kst, (((0,), (0,)), ((), ())), preferred_element_type=F32
            )
            before = before + total
        ist[h] = state
        idec[h] = jnp.broadcast_to(jnp.exp(before), (16, HEAD_DIM))
        est[h] = jnp.zeros((HEAD_DIM, HEAD_DIM), F32)
        edec[h] = jnp.ones((16, HEAD_DIM), F32)
        return 0

    lax.fori_loop(0, heads, head_local, 0)

    hops = []
    dist = 1
    while dist < E:
        hops.append(dist)
        dist *= 2
    hop_copy = [
        remote(ksend.at[r], krecv.at[r], (lax.rem(me + d, E), t)) for r, d in enumerate(hops)
    ]

    def hop_send(r):
        @pl.when(me + hops[r] < E)
        def _():
            ksend[r, :, 0:HEAD_DIM, :] = ist[...].astype(BF16)
            ksend[r, :, HEAD_DIM:HEAD_DIM + 16, :] = idec[...].astype(BF16)
            hop_copy[r].start()

    def hop_recv(r):
        @pl.when(me >= hops[r])
        def _():
            hop_copy[r].wait_recv()
            s = krecv[r, :, 0:HEAD_DIM, :].astype(F32)
            d = krecv[r, :, HEAD_DIM:HEAD_DIM + 16, :].astype(F32)
            est[...] = edec[:, 0:1, :] * s + est[...]
            edec[...] = edec[...] * d
            if r + 1 < len(hops):
                ist[...] = idec[:, 0:1, :] * s + ist[...]
                idec[...] = idec[...] * d

    hop_send(0)

    ag_partner, ag_cross, rs_partner, rs_cross, back = {}, {}, {}, {}, {}

    def piece_rows(p):
        a, n = pieces[p]
        return pl.ds(a * cap, n * cap)

    def gather_start(p):
        a, n = pieces[p]
        for k in range(max(a, 1), a + n):
            dispatch[k].wait_recv()
        rr = piece_rows(p)
        for j in range(1, G):
            ag_cross[p, j] = remote(feats.at[t, rr], feats.at[t, rr], (me, 2 * flip(g, j) + c))
            ag_cross[p, j].start()
            sent.append(ag_cross[p, j])
        for j in range(G):
            idx = 2 * flip(g, j) + c
            ag_partner[p, j] = (
                used[0], remote(feats.at[idx, rr], feats.at[idx, rr], (me, 2 * g + oc))
            )
        ag_partner[p, 0][1].start()
        sent.append(ag_partner[p, 0][1])

    def gather_relay(p):
        rr = piece_rows(p)
        for j in range(1, G):
            ag_cross[p, j].wait_recv()
            ag_partner[p, j][1].start()
            sent.append(ag_partner[p, j][1])

    def gather_end(p):
        for j in range(G):
            ag_partner[p, j][1].wait_recv()

    tile = min(256, FFl)

    def experts(p):
        a, n = pieces[p]
        rs = slice(a * cap, (a + n) * cap)

        def one(i, _):
            cc = pl.ds(pl.multiple_of(i * tile, tile), tile)
            ga = jnp.zeros((n * cap, tile), F32)
            ua = jnp.zeros((n * cap, tile), F32)
            for d in range(T):
                xs = feats[d, rs, :]
                ga += jnp.dot(xs, gate[d * Dl:(d + 1) * Dl, cc], preferred_element_type=F32)
                ua += jnp.dot(xs, up[d * Dl:(d + 1) * Dl, cc], preferred_element_type=F32)
            hidden[rs, cc] = (jax.nn.silu(ga) * ua).astype(BF16)
            return 0

        lax.fori_loop(0, FFl // tile, one, 0)

        def down_group(cls, gg):
            ff = pl.ds(pl.multiple_of((2 * gg + cls) * Dl, 128), Dl)
            part[cls, gg, rs, :] = lax.dot_general(
                hidden[rs, :], down[ff, :], (((1,), (1,)), ((), ())),
                preferred_element_type=F32,
            ).astype(BF16)

        def theirs(gg, _):
            down_group(oc, gg)
            return 0

        def ours(gg, _):
            down_group(c, gg)
            return 0

        lax.fori_loop(0, G, theirs, 0)
        rr = piece_rows(p)
        rs_partner[p] = remote(part.at[oc, :, rr], precv.at[:, rr], (me, 2 * g + oc))
        rs_partner[p].start()
        sent.append(rs_partner[p])
        lax.fori_loop(0, G, ours, 0)

    def scatter_cross(p):
        a, n = pieces[p]
        rs = slice(a * cap, (a + n) * cap)
        rr = piece_rows(p)
        rs_partner[p].wait_recv()
        for j in range(1, G):
            gj = flip(g, j)
            xsend[j - 1, rs, :] = (
                part[c, gj, rs, :].astype(F32) + precv[gj, rs, :].astype(F32)
            ).astype(BF16)
            rs_cross[p, j] = remote(
                xsend.at[j - 1, rr], xrecv.at[j - 1, rr], (me, 2 * gj + c)
            )
            rs_cross[p, j].start()
            sent.append(rs_cross[p, j])

    def give_back(p):
        a, n = pieces[p]
        rs = slice(a * cap, (a + n) * cap)
        total = part[c, g, rs, :].astype(F32) + precv[g, rs, :].astype(F32)
        for j in range(1, G):
            rs_cross[p, j].wait_recv()
            total += xrecv[j - 1, rs, :].astype(F32)
        fin[rs, :] = total.astype(BF16)
        for k in range(max(a, 1), a + n):
            block = pl.ds(k * cap, cap)
            back[k] = remote(fin.at[block], ret.at[block], (flip(me, k), t))
            back[k].start()
            sent.append(back[k])
        if a == 0:
            ret[0:cap, :] = fin[0:cap, :]

    def mixer_end():
        for load in loads[3:]:
            load.wait()
        for h in range(heads):
            lanes = slice(h * HEAD_DIM, (h + 1) * HEAD_DIM)
            r = rec[:, lanes] + lax.dot_general(
                qg[:, lanes], est[h].astype(BF16), (((1,), (1,)), ((), ())),
                preferred_element_type=F32,
            )
            r = r * lax.rsqrt(jnp.mean(r * r, axis=-1, keepdims=True) + 1e-06)
            mhid[:, lanes] = (
                r * hscale_ref[:, lanes] * jax.nn.silu(o_ref[:, lanes].astype(F32))
            ).astype(BF16)
        R = mix_out.shape[0]
        wide = mixw.shape[1]
        step = min(512, wide)

        def one(i, _):
            cc = pl.ds(pl.multiple_of(i * step, step), step)
            y = jnp.dot(mhid[...], mixw[:, cc], preferred_element_type=F32).astype(BF16)
            for d in range(T):
                mpart[d % 2, d // 2, :, cc] = y[d * R:(d + 1) * R, :]
            return 0

        lax.fori_loop(0, wide // step, one, 0)
        rs_partner["m"] = remote(mpart.at[oc], mprecv, (me, 2 * g + oc))
        rs_partner["m"].start()
        sent.append(rs_partner["m"])

    def mixer_cross():
        rs_partner["m"].wait_recv()
        for j in range(1, G):
            gj = flip(g, j)
            mxsend[j - 1] = (mpart[c, gj].astype(F32) + mprecv[gj].astype(F32)).astype(BF16)
            rs_cross["m", j] = remote(mxsend.at[j - 1], mxrecv.at[j - 1], (me, 2 * gj + c))
            rs_cross["m", j].start()
            sent.append(rs_cross["m", j])

    def mixer_out():
        total = mpart[c, g].astype(F32) + mprecv[g].astype(F32)
        for j in range(1, G):
            rs_cross["m", j].wait_recv()
            total += mxrecv[j - 1].astype(F32)
        mix_out[...] = total.astype(BF16)

    last = len(pieces) - 1
    gather_start(0)
    hop_recv(0)
    if len(hops) > 1:
        hop_send(1)
    gather_relay(0)
    for load in loads[:3]:
        load.wait()
    for p in range(len(pieces)):
        if p < last:
            gather_start(p + 1)
        gather_end(p)
        if p == 0:
            for r in range(1, len(hops)):
                hop_recv(r)
                if r + 1 < len(hops):
                    hop_send(r + 1)
        if p > 0:
            scatter_cross(p - 1)
        experts(p)
        if p < last:
            gather_relay(p + 1)
        if p > 0:
            give_back(p - 1)
    scatter_cross(last)
    mixer_end()
    give_back(last)
    mixer_cross()
    mixer_out()
    for k in range(1, E):
        back[k].wait_recv()
    exp_out[...] = lax.dot_general(
        wmat[...], ret[...], (((0,), (0,)), ((), ())), preferred_element_type=F32
    ).astype(BF16)
    for copy in sent:
        copy.wait_send()
    for r in range(len(hops)):
        @pl.when(me + hops[r] < E)
        def _():
            hop_copy[r].wait_send()


def body(E, T, q, f, v, o, gap, extra, hscale, mixw, tok, escale, routes, scores, gate, up, down):
    tokens, width = q.shape
    ntok, D = tok.shape
    heads = width // HEAD_DIM
    G = T // 2
    cap = -(-(3 * ntok // E) // 16) * 16
    S = E * cap
    Dl = D // T
    FFl = gate.shape[2]
    R = tokens // T
    half = E // 2
    pieces = ((0, half), (half, half))
    nhops = max(1, (E - 1).bit_length())
    copies = 2 * (E - 1) + nhops + len(pieces) * (G - 1 + G + 1 + G - 1) + G
    vm = pl.BlockSpec(memory_space=pltpu.VMEM)
    anyspace = pl.BlockSpec(memory_space=pl.ANY)
    V = pltpu.VMEM
    scratch = [
        V((D, FFl), BF16), V((D, FFl), BF16), V((D, FFl), BF16), V(mixw.shape, BF16),
        V((ntok, Dl), BF16), V((S, ntok), BF16), V((S, ntok), BF16), V((S, Dl), BF16),
        V((T, S, Dl), BF16), V((S, FFl), BF16), V((2, G, S, Dl), BF16), V((G, S, Dl), BF16),
        V((max(G - 1, 1), S, Dl), BF16), V((max(G - 1, 1), S, Dl), BF16),
        V((S, Dl), BF16), V((S, Dl), BF16),
        V((tokens, width), F32), V((tokens, width), F32), V((tokens, width), F32),
        V((tokens, width), BF16), V((tokens, width), F32),
        V((heads, HEAD_DIM, HEAD_DIM), F32), V((heads, 16, HEAD_DIM), F32),
        V((heads, HEAD_DIM, HEAD_DIM), F32), V((heads, 16, HEAD_DIM), F32),
        V((nhops, heads, HEAD_DIM + 16, HEAD_DIM), BF16),
        V((nhops, heads, HEAD_DIM + 16, HEAD_DIM), BF16),
        V((tokens, width), BF16), V((2, G, R, D), BF16), V((G, R, D), BF16),
        V((max(G - 1, 1), R, D), BF16), V((max(G - 1, 1), R, D), BF16),
        pltpu.SemaphoreType.DMA((4,)),
        pltpu.SemaphoreType.DMA((copies,)),
        pltpu.SemaphoreType.DMA((copies,)),
    ]
    return pl.pallas_call(
        functools.partial(kernel, E, T, cap, pieces),
        out_shape=(
            jax.ShapeDtypeStruct((R, D), BF16),
            jax.ShapeDtypeStruct((ntok, Dl), BF16),
        ),
        in_specs=[vm] * 7 + [anyspace] + [vm] * 4 + [anyspace] * 3,
        out_specs=(vm, vm),
        scratch_shapes=scratch,
        compiler_params=pltpu.CompilerParams(
            collective_id=0, has_side_effects=True, vmem_limit_bytes=60 * 1024 * 1024
        ),
    )(
        q, f, v, o, gap[None], extra, hscale[None], mixw, tok, escale[None],
        routes.T, scores.T, gate[0], up[0], down[0],
    )


def solution(mesh):
    E, T = mesh.shape["ep"], mesh.shape["tp"]
    return jax.shard_map(
        functools.partial(body, E, T),
        mesh=mesh,
        in_specs=(
            P("ep", "tp"),
            P("ep", "tp"),
            P("ep", "tp"),
            P("ep", "tp"),
            P("tp"),
            P("ep", "tp"),
            P("tp"),
            P("tp", None),
            P("ep", None),
            P(),
            P("ep", None),
            P("ep", None),
            P("ep", None, "tp"),
            P("ep", None, "tp"),
            P("ep", None, "tp"),
        ),
        out_specs=(P(("ep", "tp"), None), P("ep", "tp")),
        check_vma=False,
    )
```

time: 201 us -> 87.1 us (0.43)
  Pallas kernels: 0 us -> 81.9 us
  waiting for transfers between devices: 62.5 us -> 0 us
  blocking collectives: 54.2 us -> 0 us
  matrix products: 22.6 us -> 0 us
  local copies, waits for them, and re-layouts: 25.1 us -> 3.34 us
  other arithmetic: 16.3 us -> 0 us
  between operations: 14.1 us -> 0.64 us
  starting transfers between devices: 5.85 us -> 0 us
    pallas_call x0 -> x1, Pallas kernels: none -> 81.9 us  [body(): pl.pallas_call(functools.partial(kernel, E, T, cap, pieces), out_shape=(j...]
    reduce_scatter x2 -> x0, waiting for transfers between devices: 31.4 us -> none  [the longest x1 31.4 us: expert_half(): lax.psum_scatter(lax.dot_general(local_down, hidden, (((1,), (1,)), ((),...]
    all_to_all x1 -> x0, blocking collectives: 27.3 us -> none  [expert_half(): lax.all_to_all(outgoing, 'ep', split_axis=0, concat_axis=0, tiled=True)]
    all_gather x1 -> x0, blocking collectives: 26.8 us -> none  [entering(): lax.all_gather(a.astype(kind), axis)]
    dot_general x8 -> x0, matrix products: 22.6 us -> none  [the longest x1 6.28 us: expert_half(): up_act = jnp.dot(features, local_up, preferred_element_type=jnp.float32)]
    all_to_all x1 -> x0, waiting for transfers between devices: 19.9 us -> none  [expert_half(): lax.all_to_all(summed, 'ep', split_axis=1, concat_axis=1, tiled=True)]
    all_gather x2 -> x0, waiting for transfers between devices: 11.1 us -> none  [the longest x1 11.1 us: expert_half(): features = lax.all_gather(arrived, 'tp', axis=1, tiled=True)]
    reduce_sum x4 -> x0, other arithmetic: 6.49 us -> none  [the longest x1 2.91 us: expert_half(): variance = jnp.mean(centred * centred, axis=-1, keepdims=True)]
  transfers between devices with their start and end apart: 5 -> 0, of which waited for: 3 -> 0; matrix products, arithmetic and copies ran while one was open for 23% -> 0% of each run, Pallas kernels for 0% -> 0%
where the time goes in v1:
time: 87.1 us; the launch traced here: 85.9 us
  Pallas kernels  81.9 us (94%)
  local copies, waits for them, and re-layouts  3.34 us (4%)
    pallas_call x1, Pallas kernels, body(): pl.pallas_call(functools.partial(kernel, E, T, cap, pieces), out_shape=(j...  81.9 us
    unnamed x2, local copies, waits for them, and re-layouts  3.34 us

profile of v1, /device:TPU:0, one launch (start us, length us, event | category | flops | bytes accessed | tf_op | source)
XLA Modules:
  0.0 85.9 jit_solution(5117801842729272636)
XLA Ops:
  0.6 81.9 %shard_map.158 = (bf16[64,2048]{1,0:T(8,128)(2,1)}, bf16[256,512]{1,0:T(8,128)(2,1)}) custom-call(bf16[256,512]{1,0:T(8,128)(2,1)} %q_ref.1, bf16[256,512]{1,0:T(8,128)(2,1)} %f_ref.1, bf16[256,512]{1,0:T(8,128)(2,1)} %v_ref.1, bf16[256,512]{1,0:T(8,128)(2,1)} %o_ref.1, f32[1,512]{1,0:T(1,128)} %bitcast.12, f32[256,512]{1,0:T(8,128)} %extra_ref.1, ...), custom_call_target="tpu_custom_call" | custom-call | tf_op jit(solution)/shard_map/pallas_call | solution.py:433
  82.5 1.7 %copy.19 = bf16[64,2048]{1,0:T(8,128)(2,1)} copy(bf16[64,2048]{1,0:T(8,128)(2,1)} %get-tuple-element.4) | data formatting | bytes 524288
  84.2 1.7 %copy.20 = bf16[256,512]{1,0:T(8,128)(2,1)} copy(bf16[256,512]{1,0:T(8,128)(2,1)} %get-tuple-element.5) | data formatting | bytes 524288

commit v2 on v1

--- a/solution.py
+++ b/solution.py
@@ -72,12 +72,6 @@
         return pltpu.make_async_remote_copy(
             src_ref=src, dst_ref=dst, send_sem=send_sem.at[slot], recv_sem=recv_sem.at[slot],
             device_id=device, device_id_type=MESH,
-        )
-
-    def arrival(src, dst, copy_slot):
-        return pltpu.make_async_remote_copy(
-            src_ref=src, dst_ref=dst, send_sem=send_sem.at[copy_slot],
-            recv_sem=recv_sem.at[copy_slot], device_id=(me, t), device_id_type=MESH,
         )
 
     sent = []
@@ -354,6 +348,7 @@
         mix_out[...] = total.astype(BF16)
 
     last = len(pieces) - 1
+    hop_next = 1
     gather_start(0)
     hop_recv(0)
     if len(hops) > 1:
@@ -365,11 +360,6 @@
         if p < last:
             gather_start(p + 1)
         gather_end(p)
-        if p == 0:
-            for r in range(1, len(hops)):
-                hop_recv(r)
-                if r + 1 < len(hops):
-                    hop_send(r + 1)
         if p > 0:
             scatter_cross(p - 1)
         experts(p)
@@ -377,7 +367,15 @@
             gather_relay(p + 1)
         if p > 0:
             give_back(p - 1)
+        if p + 2 < len(hops) and p < last:
+            hop_recv(p + 1)
+            hop_send(p + 2)
+            hop_next = p + 2
     scatter_cross(last)
+    for r in range(hop_next, len(hops)):
+        hop_recv(r)
+        if r + 1 < len(hops):
+            hop_send(r + 1)
     mixer_end()
     give_back(last)
     mixer_cross()
@@ -405,8 +403,8 @@
     Dl = D // T
     FFl = gate.shape[2]
     R = tokens // T
-    half = E // 2
-    pieces = ((0, half), (half, half))
+    half, quarter = E // 2, E // 4
+    pieces = ((0, half), (half, quarter), (half + quarter, quarter))
     nhops = max(1, (E - 1).bit_length())
     copies = 2 * (E - 1) + nhops + len(pieces) * (G - 1 + G + 1 + G - 1) + G
     vm = pl.BlockSpec(memory_space=pltpu.VMEM)

time: 87.1 us -> 79 us (0.907)
  the two profiles are of different devices: /device:TPU:0 before, /device:TPU:11 now
where the time goes in v2:
time: 79 us; the launch traced here: 78.7 us
  Pallas kernels  74.8 us (95%)
  local copies, waits for them, and re-layouts  3.34 us (4%)
    pallas_call x1, Pallas kernels, body(): pl.pallas_call(functools.partial(kernel, E, T, cap, pieces), out_shape=(j...  74.8 us
    unnamed x2, local copies, waits for them, and re-layouts  3.34 us

profile of v2, /device:TPU:11, one launch (start us, length us, event | category | flops | bytes accessed | tf_op | source)
XLA Modules:
  0.0 78.7 jit_solution(14882371348303009995)
XLA Ops:
  0.6 74.8 %shard_map.158 = (bf16[64,2048]{1,0:T(8,128)(2,1)}, bf16[256,512]{1,0:T(8,128)(2,1)}) custom-call(bf16[256,512]{1,0:T(8,128)(2,1)} %q_ref.1, bf16[256,512]{1,0:T(8,128)(2,1)} %f_ref.1, bf16[256,512]{1,0:T(8,128)(2,1)} %v_ref.1, bf16[256,512]{1,0:T(8,128)(2,1)} %o_ref.1, f32[1,512]{1,0:T(1,128)} %bitcast.12, f32[256,512]{1,0:T(8,128)} %extra_ref.1, ...), custom_call_target="tpu_custom_call" | custom-call | tf_op jit(solution)/shard_map/pallas_call | solution.py:431
  75.4 1.7 %copy.19 = bf16[64,2048]{1,0:T(8,128)(2,1)} copy(bf16[64,2048]{1,0:T(8,128)(2,1)} %get-tuple-element.4) | data formatting | bytes 524288
  77.1 1.7 %copy.20 = bf16[256,512]{1,0:T(8,128)(2,1)} copy(bf16[256,512]{1,0:T(8,128)(2,1)} %get-tuple-element.5) | data formatting | bytes 524288
